TPU v7x, 256 devices: a whole 4x4x8 slice. The times are simulated.
256 devices in a mesh: sp: 64 (over z, y, core), tp: 4 (over x).
Axes of the slice: x: 4, y: 4, z: 8, core: 2. Of those that a mesh axis runs over, the one named last changes fastest.
Arguments:
- stream_in: bfloat16 [16384, 2048], P(('sp', 'tp')), may hold values from -6 to 6
- queries_one: bfloat16 [16384, 1024], P('sp', 'tp'), may hold values from -120 to 120
- queries_two: bfloat16 [16384, 1024], P('sp', 'tp'), may hold values from -120 to 120
- keys_one: bfloat16 [16384, 512], P('sp', 'tp'), may hold values from -7 to 7
- keys_two: bfloat16 [16384, 512], P('sp', 'tp'), may hold values from -7 to 7
- values: bfloat16 [16384, 1024], P('sp', 'tp'), may hold values from -6 to 6
- lambdas: float32 [8], P('tp'), may hold values from 0.3 to 0.8
- head_gain: float32 [256], replicated, may hold values from 0.1 to 1.9
- out_weight: bfloat16 [2048, 2048], P('tp'), may hold values from -0.125 to 0.125
- norm_gain: float32 [2048], replicated, may hold values from 0.1 to 1.9
- expert_ids: int32 [16384, 2], P(('sp', 'tp')), may hold values from 0 to 63, all different within a row; in each aligned block of 64 rows (0 to 63, 64 to 127, ...) at most 4 rows name the same one
- route_weight: float32 [16384, 2], P(('sp', 'tp')), may hold values from 0.1 to 1
- gate_weight: bfloat16 [64, 2048, 1024], P('sp', None, 'tp'), may hold values from -0.125 to 0.125
- up_weight: bfloat16 [64, 2048, 1024], P('sp', None, 'tp'), may hold values from -0.125 to 0.125
- down_weight: bfloat16 [64, 1024, 2048], P('sp', 'tp'), may hold values from -0.1875 to 0.1875
Outputs:
- mixed: bfloat16 [16384, 2048], P(('sp', 'tp'))
Inputs may be any that keep to these rules, and one draw needn't show every extreme that they name: `expert_ids`: each row names 2 different experts. In each aligned block of 64 rows no expert is named more than 4 times, a bound that some block reaches.
All inputs are finite; a program needn't handle non-finite values.
Results may differ from a plain program's by a relative error of at most 0.013.
Values may be sent and summed in bfloat16 or wider, within the bound.
A program may use at most 128 MiB of HBM per device.

v0:
```python
import math
import jax
import jax.numpy as jnp
from jax import lax
from jax.sharding import PartitionSpec as P

HEAD_DIM = 128
VAL_DIM = 256
EPS = 1e-06
OUT_SCALE = 0.8


def cut_along(x, dim, peers):
    before, after = (x.shape[:dim], x.shape[dim + 1 :])
    return jnp.moveaxis(x.reshape(*before, peers, -1, *after), dim, 0)


def sum_at_owner(x, axis, dim):
    peers = lax.axis_size(axis)
    tiles = lax.all_to_all(cut_along(x, dim, peers), axis, 0, 0, tiled=True)
    return jnp.sum(tiles.astype(jnp.float32), axis=0)


def update_map(carried, queries, keys, vals, allowed):
    row_max, totals, accum = carried
    scores = jnp.einsum(
        "qgrd,kgd->grqk", queries, keys, preferred_element_type=jnp.float32
    ) * HEAD_DIM ** (-0.5)
    scores = jnp.where(allowed[None, None], scores, -jnp.inf)
    new_max = jnp.maximum(row_max, jnp.max(scores, axis=-1))
    safe_max = jnp.where(new_max == -jnp.inf, 0.0, new_max)
    exp_terms = jnp.exp(scores - safe_max[..., None])
    rescale = jnp.exp(row_max - safe_max)
    totals = totals * rescale + jnp.sum(exp_terms, axis=-1)
    accum = accum * rescale[..., None] + jnp.einsum(
        "grqk,kgv->grqv", exp_terms.astype(jnp.bfloat16), vals, preferred_element_type=jnp.float32
    )
    return (new_max, totals, accum)


def fold_piece(carried, piece, q_first, q_second, query_pos, shape_info):
    kv_here, head_dim, val_dim = shape_info
    piece_rows = piece.shape[0]
    key_block = math.gcd(piece_rows, 1024)
    num_blocks = piece_rows // key_block
    last_query = jnp.max(query_pos)

    def advance(block_no, carry_now):
        first_key = block_no * key_block

        def compute(carry_in):
            rows_now = lax.dynamic_slice_in_dim(piece, block_no * key_block, key_block, 0)
            key_first = rows_now[:, : kv_here * head_dim].reshape(key_block, kv_here, head_dim)
            key_second = rows_now[:, kv_here * head_dim : 2 * kv_here * head_dim].reshape(
                key_block, kv_here, head_dim
            )
            vals = rows_now[:, 2 * kv_here * head_dim :].reshape(key_block, kv_here, val_dim)
            key_pos = first_key + lax.iota(jnp.int32, key_block)
            allowed = (key_pos[None, :] <= query_pos[:, None]) & (key_pos[None, :] >= 0)
            first_map = update_map(carry_in[0:3], q_first, key_first, vals, allowed)
            second_map = update_map(carry_in[3:6], q_second, key_second, vals, allowed)
            return first_map + second_map

        def unchanged(carry_in):
            return carry_in

        return lax.cond(first_key > last_query, unchanged, compute, carry_now)

    return lax.fori_loop(0, num_blocks, advance, carried)


def shards(
    stream_in,
    queries_one,
    queries_two,
    keys_one,
    keys_two,
    values,
    lambdas,
    head_gain,
    out_weight,
    norm_gain,
    expert_ids,
    route_weight,
    gate_weight,
    up_weight,
    down_weight,
):
    rows_q = queries_one.shape[0]
    heads_here = queries_one.shape[1] // HEAD_DIM
    kv_here = keys_one.shape[1] // HEAD_DIM
    per_kv = heads_here // kv_here
    position = lax.axis_index("sp")
    query_pos = position * rows_q + lax.iota(jnp.int32, rows_q)
    q_first = queries_one.reshape(rows_q, kv_here, per_kv, HEAD_DIM)
    q_second = queries_two.reshape(rows_q, kv_here, per_kv, HEAD_DIM)
    packed = jnp.concatenate([keys_one, keys_two, values], 1)
    shape_info = (kv_here, HEAD_DIM, VAL_DIM)
    max_init = jnp.full((kv_here, per_kv, rows_q), -jnp.inf, jnp.float32)
    sum_init = jnp.zeros((kv_here, per_kv, rows_q), jnp.float32)
    acc_init = jnp.zeros((kv_here, per_kv, rows_q, VAL_DIM), jnp.float32)
    initial = (max_init, sum_init, acc_init, max_init, sum_init, acc_init)
    final = fold_piece(
        initial,
        lax.all_gather(packed, "sp", axis=0, tiled=True),
        q_first,
        q_second,
        query_pos,
        shape_info,
    )
    mix_first = final[2] / final[1][..., None]
    mix_second = final[5] / final[4][..., None]
    difference = mix_first - lambdas.reshape(kv_here, per_kv, 1, 1) * mix_second
    mean_sq = jnp.mean(difference * difference, axis=-1, keepdims=True)
    normed_heads = (difference * lax.rsqrt(mean_sq + EPS) * head_gain * OUT_SCALE).astype(
        jnp.bfloat16
    )
    heads_out = normed_heads.transpose(2, 0, 1, 3).reshape(rows_q, heads_here * VAL_DIM)
    rows_here = stream_in.shape[0]
    picked_rows = heads_out
    attended = sum_at_owner(
        jnp.dot(picked_rows, out_weight, preferred_element_type=jnp.float32).astype(jnp.bfloat16),
        "tp",
        0,
    )
    stream = stream_in.astype(jnp.float32) + attended
    normed = (
        stream * lax.rsqrt(jnp.mean(stream * stream, axis=-1, keepdims=True) + EPS) * norm_gain
    ).astype(jnp.bfloat16)
    top_count = expert_ids.shape[1]
    experts_all = lax.axis_size("sp")
    slot_cap = 2 * top_count * rows_here // experts_all
    flat_ids = expert_ids.reshape(-1)
    one_hot = (flat_ids[:, None] == lax.iota(jnp.int32, experts_all)[None, :]).astype(jnp.int32)
    ranks = jnp.sum((jnp.cumsum(one_hot, axis=0) - 1) * one_hot, axis=1)
    slots = flat_ids * slot_cap + ranks
    selector = (slots[None, :] == lax.iota(jnp.int32, experts_all * slot_cap)[:, None]).astype(
        jnp.bfloat16
    )
    selector = jnp.sum(selector.reshape(experts_all * slot_cap, rows_here, top_count), axis=2)
    send_rows = jnp.dot(selector, normed, preferred_element_type=jnp.float32).astype(jnp.bfloat16)
    received = lax.all_to_all(send_rows, "sp", split_axis=0, concat_axis=0, tiled=True)
    all_rows = lax.all_gather(received, "tp", axis=0, tiled=True)
    picked_rows = all_rows
    gate = jnp.dot(picked_rows, gate_weight[0], preferred_element_type=jnp.float32)
    upper = jnp.dot(picked_rows, up_weight[0], preferred_element_type=jnp.float32)
    hidden = (jax.nn.silu(gate) * upper).astype(jnp.bfloat16)
    summed = lax.psum_scatter(
        jnp.dot(hidden, down_weight[0], preferred_element_type=jnp.float32).astype(jnp.bfloat16),
        "tp",
        scatter_dimension=0,
        tiled=True,
    )
    returned = lax.all_to_all(summed, "sp", split_axis=0, concat_axis=0, tiled=True)
    picked = jnp.take(returned, slots, axis=0).reshape(rows_here, top_count, -1).astype(jnp.float32)
    routed = jnp.sum(picked * route_weight[:, :, None], axis=1)
    return (stream + routed).astype(jnp.bfloat16)


def solution(mesh):
    return jax.shard_map(
        shards,
        mesh=mesh,
        in_specs=(
            P(("sp", "tp"), None),
            P("sp", "tp"),
            P("sp", "tp"),
            P("sp", "tp"),
            P("sp", "tp"),
            P("sp", "tp"),
            P("tp"),
            P(),
            P("tp", None),
            P(),
            P(("sp", "tp"), None),
            P(("sp", "tp"), None),
            P("sp", None, "tp"),
            P("sp", None, "tp"),
            P("sp", "tp", None),
        ),
        out_specs=P(("sp", "tp"), None),
        check_vma=False,
    )
```

profile of v0, /device:TPU:1, one launch (start us, length us, event | category | flops | bytes accessed | tf_op | source)
XLA Modules:
  0.0 467.8 jit_solution(7342264499680508700)
XLA Ops:
  6.5 1.8 pad_maximum_fusion
  11.4 102.2 %all-gather.3.cloned.1.call-done = bf16[16384,512]{1,0:T(8,128)(2,1)} async-done(((bf16[256,512]{1,0:T(8,128)(2,1)}), bf16[16384,512]{1,0:T(8,128)(2,1)}) %all-gather.3.cloned.1.call-update) | async-done | bytes 16777232 | tf_op jit(solution)/shard_map/all_gather | solution.py:105
  113.7 19.9 %while.24 = (s32[]{:T(128)}, f32[1,2,256]{2,1,0:T(2,128)S(1)}, f32[1,2,256]{2,1,0:T(2,128)S(1)}, f32[1,2,256,256]{3,2,1,0:T(8,128)S(1)}, f32[1,2,256]{2,1,0:T(2,...) while((s32[]{:T(128)}, f32[1,2,256]{2,1,0:T(2,128)S(1)}, ...), condition=%wide.region_8.9_spmd.clone, body=%wide.region_1.8_spmd.clone.sunk | while | flops 813707520 | bytes 17390044 | solution.py:69
  114.4 7.3 %conditional.3 = (f32[1,2,256]{2,1,0:T(2,128)S(1)}, f32[1,2,256]{2,1,0:T(2,128)S(1)}, f32[1,2,256,256]{3,2,1,0:T(8,128)S(1)}, f32[1,2,256]{2,1,0:T(2,128)S(1)}, ...) conditional(s32[]{:T(128)} %convert_element_type.98, (s32[]{:T(128)}, s32[]{:T(128)}, s32[]{:T(128)}, ...), branch_computations={%region_2.6_spmd, %region_7.7_spmd} | conditional | flops 813707520 | bytes 17380510 | solution.py:67
  114.8 1.4 fusion.43
  116.6 1.7 fusion.7
  118.2 1.4 fusion.42
  119.7 1.7 fusion.6
  136.2 1.7 convolution_convert_fusion.1
  137.9 4.1 all-to-all-start
  143.1 13.6 %all-to-all-done = bf16[4,64,2048]{2,1,0:T(8,128)(2,1)S(1)} async-done(((bf16[4,64,2048]{2,1,0:T(8,128)(2,1)}), bf16[4,64,2048]{2,1,0:T(8,128)(2,1)S(1)}, u32[]{:S(2)}, u32[]{:S(2)}) %all-to-all-start) | async-done | bytes 1048608 | tf_op jit(solution)/shard_map/all_to_all | solution.py:20
  158.1 1.2 all_to_all.20
  159.4 142.1 %all_to_all.29 = bf16[64,4,2048]{2,1,0:T(4,128)(2,1)S(1)} all-to-all(bf16[64,4,2048]{2,1,0:T(4,128)(2,1)} %all_to_all.20), channel_id=1, replica_groups=mesh['sp'=64,'tp'=4] {'sp'}, dimensions={0} | all-to-all | bytes 2097152 | tf_op jit(solution)/shard_map/all_to_all | solution.py:142
  302.9 45.5 %all-gather.5.cloned.1.call-done = bf16[1024,2048]{1,0:T(8,128)(2,1)} async-done(((bf16[256,2048]{1,0:T(8,128)(2,1)}), bf16[1024,2048]{1,0:T(8,128)(2,1)}) %all-gather.5.cloned.1.call-update) | async-done | bytes 4194320 | tf_op jit(solution)/shard_map/all_gather | solution.py:143
  348.4 4.8 %fusion.25 = f32[1024,256]{1,0:T(8,128)} fusion(bf16[1024,2048]{1,0:T(8,128)(2,1)} %all-gather.5.cloned.1.call-done, bf16[1,2048,256]{2,1,0:T(8,128)(2,1)} %param.31), kind=kOutput, calls=%fused_computation.48 | convolution fusion | flops 1073741824 | bytes 6291456 | tf_op jit(solution)/shard_map/dot_general | solution.py:145
  353.2 9.1 %convolution_convert_fusion = bf16[1024,2048]{1,0:T(8,128)(2,1)} fusion(bf16[1024,2048]{1,0:T(8,128)(2,1)} %all-gather.5.cloned.1.call-done, bf16[1,256,2048]{2,1,0:T(8,128)(2,1)S(1)} %copy-done.9, bf16[1,2048,256]{2,1,0:T(8,128)(2,1)} %param.32, f32[1024,256]{1,0:T(8,128)} %fusion.25), kind=kOutput, calls=%fused_computation.40 | convolution fusion | flops 2151153664 | bytes 11534336 | tf_op jit(solution)/shard_map/dot_general | solution.py:149
  362.4 50.0 %reduce-scatter.2.cloned.1.call-done = bf16[256,2048]{1,0:T(8,128)(2,1)} async-done(((bf16[1024,2048]{1,0:T(8,128)(2,1)}), bf16[256,2048]{1,0:T(8,128)(2,1)}) %reduce-scatter.2.cloned.1.call-update) | async-done | bytes 1048592 | tf_op jit(solution)/shard_map/reduce_scatter | solution.py:148
  412.4 2.3 all_to_all.23
  414.6 10.9 %all-to-all-start.2 = ((bf16[64,4,2048]{2,1,0:T(4,128)(2,1)}), bf16[64,4,2048]{2,1,0:T(4,128)(2,1)}, u32[]{:S(2)}, u32[]{:S(2)}) async-start(bf16[64,4,2048]{2,1,0:T(4,128)(2,1)} %all_to_all.23), calls=%async_computation.3 | async-start | bytes 2097152 | tf_op jit(solution)/shard_map/all_to_all | solution.py:154
  426.1 27.6 %all-to-all-done.2 = bf16[64,4,2048]{2,1,0:T(4,128)(2,1)} async-done(((bf16[64,4,2048]{2,1,0:T(4,128)(2,1)}), bf16[64,4,2048]{2,1,0:T(4,128)(2,1)}, u32[]{:S(2)}, u32[]{:S(2)}) %all-to-all-start.2) | async-done | bytes 1048608 | tf_op jit(solution)/shard_map/all_to_all | solution.py:154
  453.7 1.3 all_to_all.25
  455.0 1.7 gather_fusion
  456.7 1.4 gather.7
  458.2 2.3 multiply_reduce_fusion
  (168 shorter events, 12.5 us)
Async XLA Ops:
  6.5 129.7 %copy-start = (bf16[512,2048]{1,0:T(8,128)(2,1)S(1)}, bf16[512,2048]{1,0:T(8,128)(2,1)}, u32[]{:S(2)}) copy-start(bf16[512,2048]{1,0:T(8,128)(2,1)} %param.27) | copy-start | bytes 6291460
  6.5 107.1 %all-gather.3.cloned.1.call-start = ((), (), s32[]{:S(2)}) async-start(), calls=%async_computation.4 | async-start | bytes 17039360 | tf_op jit(solution)/shard_map/all_gather | solution.py:105
  133.6 1.2 copy-start.8
  133.6 2.4 copy-start.6
  136.2 5.8 %copy-start.4 = (s32[64,2]{0,1:T(2,128)S(1)}, s32[64,2]{0,1:T(2,128)}, u32[]{:S(2)}) copy-start(s32[64,2]{0,1:T(2,128)} %param.29) | copy-start | bytes 1540
  137.9 18.9 %copy-start.3 = (bf16[64,2048]{1,0:T(8,128)(2,1)S(1)}, bf16[64,2048]{1,0:T(8,128)(2,1)}, u32[]{:S(2)}) copy-start(bf16[64,2048]{1,0:T(8,128)(2,1)} %param.19) | copy-start | bytes 786436
  137.9 19.7 %copy-start.5 = (f32[2048]{0:T(1024)S(1)}, f32[2048]{0:T(1024)}, u32[]{:S(2)}) copy-start(f32[2048]{0:T(1024)} %param.28) | copy-start | bytes 24580
  137.9 18.7 %all-to-all-start = ((bf16[4,64,2048]{2,1,0:T(8,128)(2,1)}), bf16[4,64,2048]{2,1,0:T(8,128)(2,1)S(1)}, u32[]{:S(2)}, u32[]{:S(2)}) async-start(bf16[4,64,2048]{2,1,0:T(8,128)(2,1)} %bitcast.93), calls=%async_computation | async-start | bytes 2097152 | tf_op jit(solution)/shard_map/all_to_all | solution.py:20
  142.0 206.4 %all-gather.5.cloned.1.call-start = ((), (), s32[]{:S(2)}) async-start(), calls=%async_computation.5 | async-start | bytes 5242880 | tf_op jit(solution)/shard_map/all_gather | solution.py:143
  156.9 0.8 copy-start.1
  302.6 50.6 %copy-start.9 = (bf16[1,256,2048]{2,1,0:T(8,128)(2,1)S(1)}, bf16[1,256,2048]{2,1,0:T(8,128)(2,1)}, u32[]{:S(2)}) copy-start(bf16[1,256,2048]{2,1,0:T(8,128)(2,1)} %param.33) | copy-start | bytes 3145732
  302.7 109.7 %reduce-scatter.2.cloned.1.call-start = ((), (), s32[]{:S(2)}) async-start(), calls=%async_computation.6 | async-start | bytes 5242880 | tf_op jit(solution)/shard_map/reduce_scatter | solution.py:148
  362.3 63.5 %copy-start.7 = (f32[64,2]{0,1:T(2,128)S(1)}, f32[64,2]{0,1:T(2,128)}, u32[]{:S(2)}) copy-start(f32[64,2]{0,1:T(2,128)} %param.30) | copy-start | bytes 1540
  414.6 39.0 %all-to-all-start.2 = ((bf16[64,4,2048]{2,1,0:T(4,128)(2,1)}), bf16[64,4,2048]{2,1,0:T(4,128)(2,1)}, u32[]{:S(2)}, u32[]{:S(2)}) async-start(bf16[64,4,2048]{2,1,0:T(4,128)(2,1)} %all_to_all.23), calls=%async_computation.3 | async-start | bytes 2097152 | tf_op jit(solution)/shard_map/all_to_all | solution.py:154
  456.7 3.8 copy-start.2
Sparse Core Ops, SparseCore 0:
  10.1 103.4 all-gather.2
  302.8 45.6 all-gather.4
  362.5 49.8 reduce-scatter.1
where the time goes:
time: 471 us; the launch traced here: 468 us
  waiting for transfers between devices  239 us (51%)
  blocking collectives  142 us (30%)
  matrix products  22.3 us (5%)
  starting transfers between devices  15.3 us (3%)
  local copies, waits for them, and re-layouts  14.3 us (3%)
  between operations  13.4 us (3%)
  loops' own time  12.5 us (3%)
  other arithmetic  8.84 us (2%)
    all_to_all x1, blocking collectives, shards(): lax.all_to_all(send_rows, 'sp', split_axis=0, concat_axis=0, tiled=True)  142 us
    all_gather x1, waiting for transfers between devices, shards(): lax.all_gather(packed, 'sp', axis=0, tiled=True)  102 us
    reduce_scatter x1, waiting for transfers between devices, shards(): lax.psum_scatter(jnp.dot(hidden, down_weight[0], preferred_element_type=j...  50 us
    all_gather x1, waiting for transfers between devices, shards(): all_rows = lax.all_gather(received, 'tp', axis=0, tiled=True)  45.5 us
    all_to_all x1, waiting for transfers between devices, shards(): lax.all_to_all(summed, 'sp', split_axis=0, concat_axis=0, tiled=True)  27.6 us
    all_to_all x1, waiting for transfers between devices, sum_at_owner(): tiles = lax.all_to_all(cut_along(x, dim, peers), axis, 0, 0, tiled=True)  13.6 us
    another operation x1, loops' own time, fold_piece(): return lax.fori_loop(0, num_blocks, advance, carried)  11.8 us
    all_to_all x1, starting transfers between devices, shards(): lax.all_to_all(summed, 'sp', split_axis=0, concat_axis=0, tiled=True)  10.9 us
  transfers between devices with their start and end apart: 5, of which 5 were waited for; matrix products, arithmetic and copies ran while one was open for 1% of the time, Pallas kernels for 0%

commit v1 on v0

--- a/solution.py
+++ b/solution.py
@@ -102,7 +102,9 @@
     initial = (max_init, sum_init, acc_init, max_init, sum_init, acc_init)
     final = fold_piece(
         initial,
-        lax.all_gather(packed, "sp", axis=0, tiled=True),
+        jnp.concatenate(
+            lax.all_to_all(jnp.stack([packed] * lax.axis_size("sp")), "sp", 0, 0), axis=0
+        ),
         q_first,
         q_second,
         query_pos,

time: 471 us -> 814 us (1.73)
  waiting for transfers between devices: 239 us -> 498 us
  blocking collectives: 142 us -> 200 us
  starting transfers between devices: 15.3 us -> 29 us
  local copies, waits for them, and re-layouts: 14.3 us -> 23.2 us
    all_to_all x0 -> x1, waiting for transfers between devices: none -> 361 us  [shards(): lax.all_to_all(jnp.stack([packed] * lax.axis_size('sp')), 'sp', 0, 0)]
    all_gather x1 -> x0, waiting for transfers between devices: 102 us -> none  [shards(): lax.all_gather(packed, 'sp', axis=0, tiled=True)]
    all_to_all x1, blocking collectives: 142 us -> 200 us  [shards(): lax.all_to_all(send_rows, 'sp', split_axis=0, concat_axis=0, tiled=True)]
    all_to_all x0 -> x1, starting transfers between devices: none -> 13.5 us  [shards(): lax.all_to_all(jnp.stack([packed] * lax.axis_size('sp')), 'sp', 0, 0)]
  transfers between devices with their start and end apart: 5 -> 5, of which waited for: 5 -> 5; matrix products, arithmetic and copies ran while one was open for 1% -> 0% of each run, Pallas kernels for 0% -> 0%
where the time goes in v1:
time: 814 us; the launch traced here: 811 us
  waiting for transfers between devices  498 us (61%)
  blocking collectives  200 us (25%)
  starting transfers between devices  29 us (4%)
  matrix products  25.5 us (3%)
  local copies, waits for them, and re-layouts  23.2 us (3%)
  between operations  13.7 us (2%)
  other arithmetic  11 us (1%)
  loops' own time  10.1 us (1%)
    all_to_all x1, waiting for transfers between devices, shards(): lax.all_to_all(jnp.stack([packed] * lax.axis_size('sp')), 'sp', 0, 0)  361 us
    all_to_all x1, blocking collectives, shards(): lax.all_to_all(send_rows, 'sp', split_axis=0, concat_axis=0, tiled=True)  200 us
    reduce_scatter x1, waiting for transfers between devices, shards(): lax.psum_scatter(jnp.dot(hidden, down_weight[0], preferred_element_type=j...  50 us
    all_gather x1, waiting for transfers between devices, shards(): all_rows = lax.all_gather(received, 'tp', axis=0, tiled=True)  45.5 us
    all_to_all x1, waiting for transfers between devices, shards(): lax.all_to_all(summed, 'sp', split_axis=0, concat_axis=0, tiled=True)  27.6 us
  transfers between devices with their start and end apart: 5, of which 5 were waited for; matrix products, arithmetic and copies ran while one was open for 0% of the time, Pallas kernels for 0%

profile of v1, /device:TPU:1, one launch (start us, length us, event | category | flops | bytes accessed | tf_op | source)
XLA Modules:
  0.0 810.6 jit_solution(5371622345128150664)
XLA Ops:
  7.7 6.1 stack.2
  13.7 13.5 %all-to-all-start = ((bf16[64,256,512]{2,1,0:T(8,128)(2,1)}), bf16[64,256,512]{2,1,0:T(8,128)(2,1)}, u32[]{:S(2)}, u32[]{:S(2)}) async-start(bf16[64,256,512]{2,1,0:T(8,128)(2,1)} %stack.2), calls=%async_computation | async-start | bytes 33554432 | tf_op jit(solution)/shard_map/all_to_all | solution.py:106
  28.9 360.8 %all-to-all-done = bf16[64,256,512]{2,1,0:T(8,128)(2,1)} async-done(((bf16[64,256,512]{2,1,0:T(8,128)(2,1)}), bf16[64,256,512]{2,1,0:T(8,128)(2,1)}, u32[]{:S(2)}, u32[]{:S(2)}) %all-to-all-start) | async-done | bytes 16777248 | tf_op jit(solution)/shard_map/all_to_all | solution.py:106
  391.0 21.0 %while.24 = (s32[]{:T(128)}, f32[1,2,256]{2,1,0:T(2,128)S(1)}, f32[1,2,256]{2,1,0:T(2,128)}, f32[1,2,256,256]{3,2,1,0:T(8,128)S(1)}, f32[1,2,256]{2,1,0:T(2,128)...) while((s32[]{:T(128)}, f32[1,2,256]{2,1,0:T(2,128)S(1)}, ...), condition=%wide.region_8.9_spmd.clone, body=%wide.region_1.8_spmd.clone.sunk | while | flops 813707520 | bytes 26335868 | solution.py:69
  391.5 10.8 %conditional.3 = (f32[1,2,256]{2,1,0:T(2,128)S(1)}, f32[1,2,256]{2,1,0:T(2,128)}, f32[1,2,256,256]{3,2,1,0:T(8,128)S(1)}, f32[1,2,256]{2,1,0:T(2,128)S(1)}, f32[...) conditional(s32[]{:T(128)} %convert_element_type.98, (s32[]{:T(128)}, s32[]{:T(128)}, s32[]{:T(128)}, ...), branch_computations={%region_2.6_spmd, %region_7.7_spmd} | conditional | flops 813707520 | bytes 26326342 | solution.py:67
  391.9 2.7 fusion.43
  395.3 2.4 fusion.7
  399.1 1.8 fusion.6
  414.6 1.7 convolution_convert_fusion.1
  416.3 4.4 all-to-all-start.1
  421.8 14.1 %all-to-all-done.1 = bf16[4,64,2048]{2,1,0:T(8,128)(2,1)} async-done(((bf16[4,64,2048]{2,1,0:T(8,128)(2,1)}), bf16[4,64,2048]{2,1,0:T(8,128)(2,1)}, u32[]{:S(2)}, u32[]{:S(2)}) %all-to-all-start.1) | async-done | bytes 1048608 | tf_op jit(solution)/shard_map/all_to_all | solution.py:20
  439.6 1.5 all_to_all.24
  441.1 200.0 %all_to_all.34 = bf16[64,4,2048]{2,1,0:T(4,128)(2,1)} all-to-all(bf16[64,4,2048]{2,1,0:T(4,128)(2,1)S(1)} %all_to_all.24), channel_id=1, replica_groups=mesh['sp'=64,'tp'=4] {'sp'}, dimensions={0} | all-to-all | bytes 2097152 | tf_op jit(solution)/shard_map/all_to_all | solution.py:144
  641.0 2.2 all_to_all.26
  643.5 45.5 %all-gather.2.cloned.1.call-done = bf16[1024,2048]{1,0:T(8,128)(2,1)} async-done(((bf16[256,2048]{1,0:T(8,128)(2,1)}), bf16[1024,2048]{1,0:T(8,128)(2,1)}) %all-gather.2.cloned.1.call-update) | async-done | bytes 4194320 | tf_op jit(solution)/shard_map/all_gather | solution.py:145
  689.0 4.5 fusion.25
  693.5 9.4 %convolution_convert_fusion = bf16[1024,2048]{1,0:T(8,128)(2,1)} fusion(bf16[1024,2048]{1,0:T(8,128)(2,1)} %all-gather.2.cloned.1.call-done, bf16[1,256,2048]{2,1,0:T(8,128)(2,1)} %param.33, bf16[1,2048,256]{2,1,0:T(8,128)(2,1)} %param.32, f32[1024,256]{1,0:T(8,128)} %fusion.25), kind=kOutput, calls=%fused_computation.40 | convolution fusion | flops 2151153664 | bytes 11534336 | tf_op jit(solution)/shard_map/dot_general | solution.py:151
  703.0 50.0 %reduce-scatter.2.cloned.1.call-done = bf16[256,2048]{1,0:T(8,128)(2,1)} async-done(((bf16[1024,2048]{1,0:T(8,128)(2,1)}), bf16[256,2048]{1,0:T(8,128)(2,1)}) %reduce-scatter.2.cloned.1.call-update) | async-done | bytes 1048592 | tf_op jit(solution)/shard_map/reduce_scatter | solution.py:150
  752.9 2.2 all_to_all.27
  755.2 11.0 %all-to-all-start.3 = ((bf16[64,4,2048]{2,1,0:T(4,128)(2,1)}), bf16[64,4,2048]{2,1,0:T(4,128)(2,1)}, u32[]{:S(2)}, u32[]{:S(2)}) async-start(bf16[64,4,2048]{2,1,0:T(4,128)(2,1)} %all_to_all.27), calls=%async_computation.4 | async-start | bytes 2097152 | tf_op jit(solution)/shard_map/all_to_all | solution.py:156
  766.6 27.6 %all-to-all-done.3 = bf16[64,4,2048]{2,1,0:T(4,128)(2,1)} async-done(((bf16[64,4,2048]{2,1,0:T(4,128)(2,1)}), bf16[64,4,2048]{2,1,0:T(4,128)(2,1)}, u32[]{:S(2)}, u32[]{:S(2)}) %all-to-all-start.3) | async-done | bytes 1048608 | tf_op jit(solution)/shard_map/all_to_all | solution.py:156
  795.6 1.7 gather_fusion
  797.3 2.2 gather.7
  799.5 3.4 multiply_reduce_fusion
  (188 shorter events, 18.6 us)
Async XLA Ops:
  6.5 408.0 %copy-start = (bf16[512,2048]{1,0:T(8,128)(2,1)S(1)}, bf16[512,2048]{1,0:T(8,128)(2,1)}, u32[]{:S(2)}) copy-start(bf16[512,2048]{1,0:T(8,128)(2,1)} %param.27) | copy-start | bytes 6291460
  13.7 14.1 %copy-start.6 = (bf16[256,256]{1,0:T(8,128)(2,1)S(1)}, bf16[256,256]{1,0:T(8,128)(2,1)}, u32[]{:S(2)}) copy-start(bf16[256,256]{1,0:T(8,128)(2,1)} %param.20) | copy-start | bytes 393220
  13.7 14.9 %copy-start.7 = (bf16[256,256]{1,0:T(8,128)(2,1)S(1)}, bf16[256,256]{1,0:T(8,128)(2,1)}, u32[]{:S(2)}) copy-start(bf16[256,256]{1,0:T(8,128)(2,1)} %param.21) | copy-start | bytes 393220
  13.7 376.0 %all-to-all-start = ((bf16[64,256,512]{2,1,0:T(8,128)(2,1)}), bf16[64,256,512]{2,1,0:T(8,128)(2,1)}, u32[]{:S(2)}, u32[]{:S(2)}) async-start(bf16[64,256,512]{2,1,0:T(8,128)(2,1)} %stack.2), calls=%async_computation | async-start | bytes 33554432 | tf_op jit(solution)/shard_map/all_to_all | solution.py:106
  395.3 2.4 copy-start.4
  399.1 2.2 copy-start.1
  401.0 0.7 copy-start.8
  401.0 0.7 copy-start.11
  401.7 0.6 copy-start.12
  412.0 1.3 copy-start.10
  412.0 1.3 copy-start.13
  412.0 1.2 copy-start.18
  412.0 2.5 copy-start.16
  414.6 6.2 copy-start.14
  416.3 21.0 %copy-start.5 = (bf16[64,2048]{1,0:T(8,128)(2,1)S(1)}, bf16[64,2048]{1,0:T(8,128)(2,1)}, u32[]{:S(2)}) copy-start(bf16[64,2048]{1,0:T(8,128)(2,1)} %param.19) | copy-start | bytes 786436
  416.3 21.8 %copy-start.15 = (f32[2048]{0:T(1024)S(1)}, f32[2048]{0:T(1024)}, u32[]{:S(2)}) copy-start(f32[2048]{0:T(1024)} %param.28) | copy-start | bytes 24580
  416.3 19.6 %all-to-all-start.1 = ((bf16[4,64,2048]{2,1,0:T(8,128)(2,1)}), bf16[4,64,2048]{2,1,0:T(8,128)(2,1)}, u32[]{:S(2)}, u32[]{:S(2)}) async-start(bf16[4,64,2048]{2,1,0:T(8,128)(2,1)} %bitcast.28), calls=%async_computation.1 | async-start | bytes 2097152 | tf_op jit(solution)/shard_map/all_to_all | solution.py:20
  420.7 268.3 %all-gather.2.cloned.1.call-start = ((), (), s32[]{:S(2)}) async-start(), calls=%async_computation.5 | async-start | bytes 5242880 | tf_op jit(solution)/shard_map/all_gather | solution.py:145
  437.3 0.8 copy-start.2
  641.0 48.0 %copy-start.19 = (bf16[1,2048,256]{2,1,0:T(8,128)(2,1)S(1)}, bf16[1,2048,256]{2,1,0:T(8,128)(2,1)}, u32[]{:S(2)}) copy-start(bf16[1,2048,256]{2,1,0:T(8,128)(2,1)} %param.31) | copy-start | bytes 3145732
  643.3 109.7 %reduce-scatter.2.cloned.1.call-start = ((), (), s32[]{:S(2)}) async-start(), calls=%async_computation.6 | async-start | bytes 5242880 | tf_op jit(solution)/shard_map/reduce_scatter | solution.py:150
  703.0 63.6 %copy-start.17 = (f32[64,2]{0,1:T(2,128)S(1)}, f32[64,2]{0,1:T(2,128)}, u32[]{:S(2)}) copy-start(f32[64,2]{0,1:T(2,128)} %param.30) | copy-start | bytes 1540
  755.2 39.0 %all-to-all-start.3 = ((bf16[64,4,2048]{2,1,0:T(4,128)(2,1)}), bf16[64,4,2048]{2,1,0:T(4,128)(2,1)}, u32[]{:S(2)}, u32[]{:S(2)}) async-start(bf16[64,4,2048]{2,1,0:T(4,128)(2,1)} %all_to_all.27), calls=%async_computation.4 | async-start | bytes 2097152 | tf_op jit(solution)/shard_map/all_to_all | solution.py:156
  797.3 5.7 copy-start.3
  (1 other events, 0.6 us)
Sparse Core Ops, SparseCore 0:
  643.4 45.6 all-gather.1
  703.1 49.8 reduce-scatter.1
